TPU v7x, 32 devices: a whole 2x2x4 slice. The times are simulated.
32 devices in a mesh: grp: 2 (over y), sp: 4 (over z), tp: 4 (over x, core).
Axes of the slice: x: 2, y: 2, z: 4, core: 2. Of those that a mesh axis runs over, the one named last changes fastest.
Arguments:
- conv_input: bfloat16 [4096, 1024], P(('grp', 'sp'), 'tp'), parts along dimension 0, may hold values from -6 to 6
- pre_gate: bfloat16 [4096, 1024], P(('grp', 'sp'), 'tp'), parts along dimension 0, may hold values from -6 to 6
- post_gate: bfloat16 [4096, 1024], P(('grp', 'sp'), 'tp'), parts along dimension 0, may hold values from -6 to 6
- conv_taps: float32 [3, 1024], replicated, may hold values from -3.5 to 3.5
- out_proj: bfloat16 [1024, 2048], replicated, may hold values from -0.1875 to 0.1875
- residual_in: bfloat16 [4096, 2048], P(('grp', 'sp', 'tp')), parts along dimension 0, may hold values from -6 to 6
- norm_gain: float32 [2048], replicated, may hold values from 0.1 to 1.9
- routes: int32 [4096, 2], P(('grp', 'sp', 'tp')), parts along dimension 0, may hold values from 0 to 7, as said below
- route_weight: float32 [4096, 2], P(('grp', 'sp', 'tp')), parts along dimension 0, may hold values from 0.1 to 1
- w_gate: bfloat16 [8, 2048, 1024], P('sp', None, 'tp'), may hold values from -0.125 to 0.125
- w_up: bfloat16 [8, 2048, 1024], P('sp', None, 'tp'), may hold values from -0.125 to 0.125
- w_down: bfloat16 [8, 1024, 2048], P('sp', 'tp'), may hold values from -0.1875 to 0.1875
Outputs:
- layer_out: bfloat16 [4096, 2048], P(('grp', 'sp', 'tp')), parts along dimension 0
There are 2 independent parts, one for each index of `grp`. A program takes and returns all parts, laid end to end along the dimension named above; an argument that names none is the same for every part. Nothing has to cross between parts.
Inputs may be any that keep to these rules, and one draw needn't show every extreme that they name: `routes`: the two numbers of a row differ and lie in the same group of 2 consecutive experts. In each aligned block of 128 rows every expert is named exactly 32 times.
All inputs are finite; a program needn't handle non-finite values.
Results may differ from a plain program's by a relative error of at most 0.0085.
Values may be sent and summed in bfloat16 or wider, within the bound.
A program may use at most 64 MiB of HBM per device.

v0:
```python
import jax
import jax.numpy as jnp
from jax import lax
from jax.sharding import PartitionSpec as P


def shifted(block, axis, distance):
    devices = range(lax.axis_size(axis))
    route = [(i - distance, i) for i in devices if i - distance in devices]
    return lax.ppermute(block, axis, route)


def on_device(
    conv_input,
    pre_gate,
    post_gate,
    conv_taps,
    out_proj,
    residual_in,
    norm_gain,
    routes,
    route_weight,
    w_gate,
    w_up,
    w_down,
):
    shards = lax.axis_size("tp")
    place = lax.axis_index("tp")
    seq_ranks = lax.axis_size("sp")
    channels = conv_input.shape[1]
    width = residual_in.shape[1]
    taps = lax.dynamic_slice_in_dim(conv_taps, place * channels, channels, 1)
    prior_input, prior_gate = shifted((conv_input[-2:], pre_gate[-2:]), "sp", 1)
    gated = jnp.concatenate(
        [
            prior_gate.astype(jnp.float32) * prior_input.astype(jnp.float32),
            pre_gate.astype(jnp.float32) * conv_input.astype(jnp.float32),
        ],
        axis=0,
    )
    conv = gated[2:] * taps[2] + gated[1:-1] * taps[1] + gated[:-2] * taps[0]
    mixed = (post_gate.astype(jnp.float32) * conv).astype(jnp.bfloat16)
    token_rows = lax.all_to_all(mixed, "tp", split_axis=0, concat_axis=1, tiled=True)
    projected = jnp.dot(token_rows, out_proj, preferred_element_type=jnp.float32)
    stream = residual_in.astype(jnp.float32) + projected
    scale = lax.rsqrt(jnp.mean(stream * stream, axis=-1, keepdims=True) + 1e-06)
    normed = (stream * scale * norm_gain).astype(jnp.bfloat16)
    block_rows = routes.shape[0]
    local_experts = w_gate.shape[0]
    experts = local_experts * seq_ranks
    capacity = 2 * block_rows // experts
    flat_routes = routes.reshape(-1)
    position = jnp.arange(flat_routes.shape[0], dtype=jnp.int32)
    earlier = (flat_routes[:, None] == flat_routes[None, :]) & (
        position[None, :] < position[:, None]
    )
    rank = jnp.sum(earlier.astype(jnp.int32), axis=1)
    slot = flat_routes * capacity + rank
    outgoing = (
        jnp.zeros((experts * capacity, width), jnp.bfloat16).at[slot].set(normed[position // 2])
    )
    outgoing = outgoing.reshape(seq_ranks, local_experts, capacity, width)
    spread = lax.all_gather(
        lax.all_to_all(outgoing, "sp", split_axis=0, concat_axis=0, tiled=True)[:, None],
        "tp",
        axis=1,
        tiled=True,
    )
    count = spread.shape[3]
    partials = []
    for expert in range(local_experts):
        rows = spread[:, :, expert].reshape(seq_ranks * shards * count, width)
        gate = jnp.dot(rows, w_gate[expert], preferred_element_type=jnp.float32)
        upper = jnp.dot(rows, w_up[expert], preferred_element_type=jnp.float32)
        hidden = (jax.nn.silu(gate) * upper).astype(jnp.bfloat16)
        part = jnp.dot(hidden, w_down[expert], preferred_element_type=jnp.float32).astype(
            jnp.bfloat16
        )
        partials.append(part.reshape(seq_ranks, shards, count, width))
    stacked = jnp.stack(partials, axis=2)
    summed = lax.psum_scatter(stacked, "tp", scatter_dimension=1, tiled=True).astype(jnp.float32)
    returned = lax.all_to_all(
        summed[:, 0].astype(jnp.bfloat16), "sp", split_axis=0, concat_axis=0, tiled=True
    )
    results = returned.reshape(experts * capacity, width)[slot]
    results = results.reshape(block_rows, 2, width).astype(jnp.float32)
    weighted = jnp.sum(route_weight[:, :, None] * results, axis=1)
    return (stream + weighted).astype(jnp.bfloat16)


def solution(mesh):
    return jax.shard_map(
        on_device,
        mesh=mesh,
        in_specs=(
            P(("grp", "sp"), "tp"),
            P(("grp", "sp"), "tp"),
            P(("grp", "sp"), "tp"),
            P(),
            P(),
            P(("grp", "sp", "tp"), None),
            P(),
            P(("grp", "sp", "tp"), None),
            P(("grp", "sp", "tp"), None),
            P("sp", None, "tp"),
            P("sp", None, "tp"),
            P("sp", "tp", None),
        ),
        out_specs=P(("grp", "sp", "tp"), None),
        check_vma=False,
    )
```

profile of v0, /device:TPU:0, one launch (start us, length us, event | category | flops | bytes accessed | tf_op | source)
XLA Modules:
  0.0 258.8 jit_solution(13987586749709506822)
XLA Ops:
  6.5 0.7 slice.46
  7.3 4.9 %collective-permute-start = (bf16[2,256]{1,0:T(2,128)(2,1)S(1)}, bf16[2,256]{1,0:T(2,128)(2,1)S(1)}, u32[]{:S(2)}, u32[]{:S(2)}) collective-permute-start(bf16[2,256]{1,0:T(2,128)(2,1)S(1)} %slice.46), channel_id=1, source_target_pairs={{0,4},{4,8},{8,12},{1,5},{5,9},{9,13},{2,6},{6,10},{10,14},{3,7},{... | collective-permute-start | bytes 3080 | tf_op jit(solution)/shard_map/ppermute | solution.py:10
  12.2 0.7 slice.47
  12.9 3.5 %collective-permute-start.1 = (bf16[2,256]{1,0:T(2,128)(2,1)S(1)}, bf16[2,256]{1,0:T(2,128)(2,1)S(1)}, u32[]{:S(2)}, u32[]{:S(2)}) collective-permute-start(bf16[2,256]{1,0:T(2,128)(2,1)S(1)} %slice.47), channel_id=1, source_target_pairs={{0,4},{4,8},{8,12},{1,5},{5,9},{9,13},{2,6},{6,10},{10,14},{3,7},{... | collective-permute-start | bytes 3080 | tf_op jit(solution)/shard_map/ppermute | solution.py:10
  16.4 1.1 convert_multiply_fusion
  17.5 0.8 copy.32
  18.3 0.7 broadcast_multiply_fusion
  19.3 0.9 fusion.46
  20.5 1.9 fusion.27
  22.4 3.4 %all-to-all-start = ((bf16[4,128,256]{2,1,0:T(8,128)(2,1)}), bf16[4,128,256]{2,1,0:T(8,128)(2,1)S(1)}, u32[]{:S(2)}, u32[]{:S(2)}) async-start(bf16[4,128,256]{2,1,0:T(8,128)(2,1)} %bitcast.3), calls=%async_computation | async-start | bytes 524288 | tf_op jit(solution)/shard_map/all_to_all | solution.py:43
  25.8 5.9 %all-to-all-done = bf16[4,128,256]{2,1,0:T(8,128)(2,1)S(1)} async-done(((bf16[4,128,256]{2,1,0:T(8,128)(2,1)}), bf16[4,128,256]{2,1,0:T(8,128)(2,1)S(1)}, u32[]{:S(2)}, u32[]{:S(2)}) %all-to-all-start) | async-done | bytes 262176 | tf_op jit(solution)/shard_map/all_to_all | solution.py:43
  31.9 3.0 %multiply_reduce_fusion.1 = (f32[128]{0:T(128)S(1)}, f32[128,2048]{1,0:T(8,128)S(1)}) fusion(bf16[128,1024]{0,1:T(8,128)(2,1)S(1)} %bitcast.62, bf16[1024,2048]{1,0:T(8,128)(2,1)} %param.16, bf16[128,2048]{1,0:T(8,128)(2,1)S(1)} %copy-done.1), kind=kOutput, calls=%fused_computation.31 | convolution fusion | flops 537919360 | bytes 6029824 | tf_op jit(solution)/shard_map/dot_general | solution.py:44
  35.1 5.7 %scatter_custom_fusion = bf16[256,2048]{1,0:T(8,128)(2,1)S(1)} fusion(s32[256]{0:T(256)S(1)} %bitcast.67, bf16[128,2048]{1,0:T(8,128)(2,1)S(1)} %multiply_convert_fusion, s32[1024]{0:T(1024)S(1)} %pad_clamp_fusion.1, bf16[]{:T(256)} %constant.35.clone.1), kind=kCustom, calls=%fused_computation.21 | custom fusion | bytes 1048578 | tf_op jit(solution)/shard_map/scatter | solution.py:60
  40.8 28.9 %all_to_all.29 = bf16[4,2,32,2048]{3,2,1,0:T(8,128)(2,1)} all-to-all(bf16[4,2,32,2048]{3,2,1,0:T(8,128)(2,1)S(1)} %bitcast.55), channel_id=1, replica_groups=mesh['grp'=2,'sp'=4,'tp'=4] {'sp'}, dimensions={0} | all-to-all | bytes 2097152 | tf_op jit(solution)/shard_map/all_to_all | solution.py:64
  70.0 32.8 %all-gather.3.cloned.1.call-done = bf16[4,8,32,2048]{3,2,1,0:T(8,128)(2,1)} async-done(((bf16[4,2,32,2048]{3,2,1,0:T(8,128)(2,1)}), bf16[4,8,32,2048]{3,2,1,0:T(8,128)(2,1)}) %all-gather.3.cloned.1.call-update) | async-done | bytes 4194320 | tf_op jit(solution)/shard_map/all_gather | solution.py:63
  102.7 2.8 %fusion.45 = (bf16[4,4,1,32,2048]{4,3,2,1,0:T(8,128)(2,1)S(1)}, bf16[4,4,1,32,2048]{4,3,2,1,0:T(8,128)(2,1)S(1)}) fusion(bf16[4,4,2,32,2048]{4,3,2,1,0:T(8,128)(2,1)} %bitcast.54), kind=kLoop, calls=%fused_computation.73 | loop fusion | bytes 8388608 | tf_op jit(solution)/shard_map/slice | solution.py:72
  105.6 1.5 fusion.10
  107.1 1.5 fusion.5
  108.6 6.0 %convolution_convert_fusion.1 = bf16[512,2048]{1,0:T(8,128)(2,1)} fusion(bf16[512,2048]{1,0:T(8,128)(2,1)} %bitcast.59, bf16[2,256,2048]{2,1,0:T(8,128)(2,1)} %param.23, bf16[2,2048,256]{2,1,0:T(8,128)(2,1)} %param.22, f32[512,256]{1,0:T(8,128)} %fusion.10), kind=kOutput, calls=%fused_computation.5 | convolution fusion | flops 1075576832 | bytes 6815744 | tf_op jit(solution)/shard_map/dot_general | solution.py:76
  114.5 5.4 %convolution_convert_fusion = bf16[512,2048]{1,0:T(8,128)(2,1)} fusion(bf16[512,2048]{1,0:T(8,128)(2,1)S(1)} %bitcast.57, bf16[2,256,2048]{2,1,0:T(8,128)(2,1)} %param.23, bf16[2,2048,256]{2,1,0:T(8,128)(2,1)} %param.22, f32[512,256]{1,0:T(8,128)} %fusion.5), kind=kOutput, calls=%fused_computation.4 | convolution fusion | flops 1075576832 | bytes 6815744 | tf_op jit(solution)/shard_map/dot_general | solution.py:76
  119.9 4.5 %pad_maximum_fusion = bf16[4,4,2,32,2048]{4,3,1,0,2:T(8,128)(2,1)} fusion(bf16[4,4,1,32,2048]{4,3,1,0,2:T(8,128)(2,1)} %bitcast.61, bf16[4,4,1,32,2048]{4,3,1,0,2:T(8,128)(2,1)} %bitcast.60), kind=kLoop, calls=%fused_computation.3 | loop fusion | flops 2097152 | bytes 8388608 | tf_op jit(solution)/shard_map/stack | solution.py:80
  124.5 0.6 copy-done.5
  125.1 0.6 dynamic-slice
  125.7 84.4 %all-reduce.3.cloned.1.call-done = bf16[4,4,2,32,2048]{4,3,1,0,2:T(8,128)(2,1)} async-done(((bf16[4,4,2,32,2048]{4,3,1,0,2:T(8,128)(2,1)}), bf16[4,4,2,32,2048]{4,3,1,0,2:T(8,128)(2,1)}) %all-reduce.3.cloned.1.call-update) | async-done | bytes 4194320
  210.1 1.9 dynamic-slice_bitcast_fusion
  212.1 1.0 copy.33
  213.1 4.6 %all-to-all-start.2 = ((bf16[4,2,32,2048]{3,2,1,0:T(8,128)(2,1)}), bf16[4,2,32,2048]{3,2,1,0:T(8,128)(2,1)S(1)}, u32[]{:S(2)}, u32[]{:S(2)}) async-start(bf16[4,2,32,2048]{3,2,1,0:T(8,128)(2,1)} %copy.33), calls=%async_computation.2 | async-start | bytes 2097152 | tf_op jit(solution)/shard_map/all_to_all | solution.py:82
  217.8 25.3 %all-to-all-done.2 = bf16[4,2,32,2048]{3,2,1,0:T(8,128)(2,1)S(1)} async-done(((bf16[4,2,32,2048]{3,2,1,0:T(8,128)(2,1)}), bf16[4,2,32,2048]{3,2,1,0:T(8,128)(2,1)S(1)}, u32[]{:S(2)}, u32[]{:S(2)}) %all-to-all-start.2) | async-done | bytes 1048608 | tf_op jit(solution)/shard_map/all_to_all | solution.py:82
  243.1 2.3 gather_fusion
  245.5 2.4 reshape.99
  247.8 3.2 %multiply_reduce_fusion = f32[128,2048]{1,0:T(8,128)S(1)} fusion(f32[128,2,2048]{2,1,0:T(2,128)S(1)} %reshape.99, f32[128,2]{1,0:T(8,128)S(1)} %copy.30), kind=kLoop, calls=%fused_computation.7 | loop fusion | flops 786432 | bytes 3146752 | tf_op jit(solution)/shard_map/reduce_sum | solution.py:87
  251.0 0.9 add_convert_fusion
  (30 shorter events, 1.4 us)
Async XLA Ops:
  6.5 25.4 %copy-start.1 = (bf16[128,2048]{1,0:T(8,128)(2,1)S(1)}, bf16[128,2048]{1,0:T(8,128)(2,1)}, u32[]{:S(2)}) copy-start(bf16[128,2048]{1,0:T(8,128)(2,1)} %param.17) | copy-start | bytes 1572868
  7.3 13.2 %collective-permute-start = (bf16[2,256]{1,0:T(2,128)(2,1)S(1)}, bf16[2,256]{1,0:T(2,128)(2,1)S(1)}, u32[]{:S(2)}, u32[]{:S(2)}) collective-permute-start(bf16[2,256]{1,0:T(2,128)(2,1)S(1)} %slice.46), channel_id=1, source_target_pairs={{0,4},{4,8},{8,12},{1,5},{5,9},{9,13},{2,6},{6,10},{10,14},{3,7},{... | collective-permute-start | bytes 3080 | tf_op jit(solution)/shard_map/ppermute | solution.py:10
  12.9 7.5 %collective-permute-start.1 = (bf16[2,256]{1,0:T(2,128)(2,1)S(1)}, bf16[2,256]{1,0:T(2,128)(2,1)S(1)}, u32[]{:S(2)}, u32[]{:S(2)}) collective-permute-start(bf16[2,256]{1,0:T(2,128)(2,1)S(1)} %slice.47), channel_id=1, source_target_pairs={{0,4},{4,8},{8,12},{1,5},{5,9},{9,13},{2,6},{6,10},{10,14},{3,7},{... | collective-permute-start | bytes 3080 | tf_op jit(solution)/shard_map/ppermute | solution.py:10
  22.4 9.4 %all-to-all-start = ((bf16[4,128,256]{2,1,0:T(8,128)(2,1)}), bf16[4,128,256]{2,1,0:T(8,128)(2,1)S(1)}, u32[]{:S(2)}, u32[]{:S(2)}) async-start(bf16[4,128,256]{2,1,0:T(8,128)(2,1)} %bitcast.3), calls=%async_computation | async-start | bytes 524288 | tf_op jit(solution)/shard_map/all_to_all | solution.py:43
  25.8 76.9 %all-gather.3.cloned.1.call-start = ((), (), s32[]{:S(2)}) async-start(), calls=%async_computation.3 | async-start | bytes 5242880 | tf_op jit(solution)/shard_map/all_gather | solution.py:63
  31.9 3.0 %copy-start.2 = (f32[2048]{0:T(1024)S(1)}, f32[2048]{0:T(1024)}, u32[]{:S(2)}) copy-start(f32[2048]{0:T(1024)} %param.18) | copy-start | bytes 24580
  69.7 140.4 %all-reduce.3.cloned.1.call-start = ((), (), s32[]{:S(2)}) async-start(), calls=%async_computation.4 | async-start | bytes 8388608
  102.7 2.9 %copy-start.4 = (bf16[2,2048,256]{2,1,0:T(8,128)(2,1)S(1)}, bf16[2,2048,256]{2,1,0:T(8,128)(2,1)}, u32[]{:S(2)}) copy-start(bf16[2,2048,256]{2,1,0:T(8,128)(2,1)} %param.21) | copy-start | bytes 6291460
  105.5 1.6 copy-start
  124.5 0.7 copy-start.5
  212.1 5.6 %copy-start.3 = (f32[128,2]{0,1:T(2,128)S(1)}, f32[128,2]{0,1:T(2,128)}, u32[]{:S(2)}) copy-start(f32[128,2]{0,1:T(2,128)} %param.20) | copy-start | bytes 3076
  213.1 30.0 %all-to-all-start.2 = ((bf16[4,2,32,2048]{3,2,1,0:T(8,128)(2,1)}), bf16[4,2,32,2048]{3,2,1,0:T(8,128)(2,1)S(1)}, u32[]{:S(2)}, u32[]{:S(2)}) async-start(bf16[4,2,32,2048]{3,2,1,0:T(8,128)(2,1)} %copy.33), calls=%async_computation.2 | async-start | bytes 2097152 | tf_op jit(solution)/shard_map/all_to_all | solution.py:82
Sparse Core Ops, SparseCore 0:
  69.8 32.8 all-gather.2
  124.6 85.4 all-reduce.2
where the time goes:
time: 259 us
  waiting for transfers between devices  148 us (57%)
  blocking collectives  28.9 us (11%)
  local copies, waits for them, and re-layouts  21.2 us (8%)
  matrix products  17.4 us (7%)
  starting transfers between devices  16.7 us (6%)
  between operations  13.6 us (5%)
  other arithmetic  12.7 us (5%)
    unnamed x3, waiting for transfers between devices  84.5 us
    all_gather x1, waiting for transfers between devices, on_device(): lax.all_gather(lax.all_to_all(outgoing, 'sp', split_axis=0, concat_axis=0...  32.8 us
    all_to_all x1, blocking collectives, on_device(): lax.all_to_all(outgoing, 'sp', split_axis=0, concat_axis=0, tiled=True)  28.9 us
    all_to_all x1, waiting for transfers between devices, on_device(): lax.all_to_all(summed[:, 0].astype(jnp.bfloat16), 'sp', split_axis=0, con...  25.3 us
    dot_general x2, matrix products, on_device(): jnp.dot(hidden, w_down[expert], preferred_element_type=jnp.float32)  11.3 us
    ppermute x2, starting transfers between devices, shifted(): return lax.ppermute(block, axis, route)  8.42 us
    all_to_all x1, waiting for transfers between devices, on_device(): lax.all_to_all(mixed, 'tp', split_axis=0, concat_axis=1, tiled=True)  5.91 us
    scatter x1, local copies, waits for them, and re-layouts, on_device(): jnp.zeros((experts * capacity, width), jnp.bfloat16).at[slot]  5.7 us
  transfers between devices with their start and end apart: 6, of which 4 were waited for; matrix products, arithmetic and copies ran while one was open for 2% of the time, Pallas kernels for 0%

commit v1 on v0

--- a/solution.py
+++ b/solution.py
@@ -60,11 +60,17 @@
         jnp.zeros((experts * capacity, width), jnp.bfloat16).at[slot].set(normed[position // 2])
     )
     outgoing = outgoing.reshape(seq_ranks, local_experts, capacity, width)
-    spread = lax.all_gather(
-        lax.all_to_all(outgoing, "sp", split_axis=0, concat_axis=0, tiled=True)[:, None],
-        "tp",
+    spread = jnp.concatenate(
+        lax.all_to_all(
+            jnp.stack(
+                [lax.all_to_all(outgoing, "sp", split_axis=0, concat_axis=0, tiled=True)[:, None]]
+                * lax.axis_size("tp")
+            ),
+            "tp",
+            0,
+            0,
+        ),
         axis=1,
-        tiled=True,
     )
     count = spread.shape[3]
     partials = []

time: 259 us -> 275 us (1.062)
  blocking collectives: 28.9 us -> 78.8 us
  waiting for transfers between devices: 148 us -> 114 us
    all_to_all x0 -> x1, blocking collectives: none -> 50.7 us  [on_device(): lax.all_to_all(jnp.stack([lax.all_to_all(outgoing, 'sp', split_axis=0, co...]
    all_gather x1 -> x0, waiting for transfers between devices: 32.8 us -> none  [on_device(): lax.all_gather(lax.all_to_all(outgoing, 'sp', split_axis=0, concat_axis=0...]
    unnamed x3 -> x2, waiting for transfers between devices: 84.5 us -> 82.6 us
  transfers between devices with their start and end apart: 6 -> 5, of which waited for: 4 -> 3; matrix products, arithmetic and copies ran while one was open for 2% -> 2% of each run, Pallas kernels for 0% -> 0%
where the time goes in v1:
time: 275 us; the launch traced here: 274 us
  waiting for transfers between devices  114 us (41%)
  blocking collectives  78.8 us (29%)
  local copies, waits for them, and re-layouts  21.6 us (8%)
  matrix products  17.4 us (6%)
  starting transfers between devices  16.5 us (6%)
  between operations  13.6 us (5%)
  other arithmetic  12.6 us (5%)
    unnamed x2, waiting for transfers between devices  82.6 us
    all_to_all x1, blocking collectives, on_device(): lax.all_to_all(jnp.stack([lax.all_to_all(outgoing, 'sp', split_axis=0, co...  50.7 us
    all_to_all x1, blocking collectives, on_device(): lax.all_to_all(outgoing, 'sp', split_axis=0, concat_axis=0, tiled=True)  28.1 us
    all_to_all x1, waiting for transfers between devices, on_device(): lax.all_to_all(summed[:, 0].astype(jnp.bfloat16), 'sp', split_axis=0, con...  25.3 us
    dot_general x2, matrix products, on_device(): jnp.dot(hidden, w_down[expert], preferred_element_type=jnp.float32)  11.3 us
    ppermute x2, starting transfers between devices, shifted(): return lax.ppermute(block, axis, route)  8.42 us
    all_to_all x1, waiting for transfers between devices, on_device(): lax.all_to_all(mixed, 'tp', split_axis=0, concat_axis=1, tiled=True)  5.91 us
    scatter x1, local copies, waits for them, and re-layouts, on_device(): jnp.zeros((experts * capacity, width), jnp.bfloat16).at[slot]  5.7 us
  transfers between devices with their start and end apart: 5, of which 3 were waited for; matrix products, arithmetic and copies ran while one was open for 2% of the time, Pallas kernels for 0%

profile of v1, /device:TPU:0, one launch (start us, length us, event | category | flops | bytes accessed | tf_op | source)
XLA Modules:
  0.0 274.3 jit_solution(12502963136567131496)
XLA Ops:
  6.5 0.7 slice.46
  7.3 4.9 %collective-permute-start = (bf16[2,256]{1,0:T(2,128)(2,1)S(1)}, bf16[2,256]{1,0:T(2,128)(2,1)S(1)}, u32[]{:S(2)}, u32[]{:S(2)}) collective-permute-start(bf16[2,256]{1,0:T(2,128)(2,1)S(1)} %slice.46), channel_id=1, source_target_pairs={{0,4},{4,8},{8,12},{1,5},{5,9},{9,13},{2,6},{6,10},{10,14},{3,7},{... | collective-permute-start | bytes 3080 | tf_op jit(solution)/shard_map/ppermute | solution.py:10
  12.2 0.7 slice.47
  12.9 3.5 %collective-permute-start.1 = (bf16[2,256]{1,0:T(2,128)(2,1)S(1)}, bf16[2,256]{1,0:T(2,128)(2,1)S(1)}, u32[]{:S(2)}, u32[]{:S(2)}) collective-permute-start(bf16[2,256]{1,0:T(2,128)(2,1)S(1)} %slice.47), channel_id=1, source_target_pairs={{0,4},{4,8},{8,12},{1,5},{5,9},{9,13},{2,6},{6,10},{10,14},{3,7},{... | collective-permute-start | bytes 3080 | tf_op jit(solution)/shard_map/ppermute | solution.py:10
  16.4 1.1 convert_multiply_fusion
  17.5 0.8 copy.35
  18.3 0.7 broadcast_multiply_fusion
  19.3 0.9 fusion.46
  20.5 1.9 fusion.27
  22.4 3.4 %all-to-all-start = ((bf16[4,128,256]{2,1,0:T(8,128)(2,1)}), bf16[4,128,256]{2,1,0:T(8,128)(2,1)S(1)}, u32[]{:S(2)}, u32[]{:S(2)}) async-start(bf16[4,128,256]{2,1,0:T(8,128)(2,1)} %bitcast.3), calls=%async_computation | async-start | bytes 524288 | tf_op jit(solution)/shard_map/all_to_all | solution.py:43
  25.8 5.9 %all-to-all-done = bf16[4,128,256]{2,1,0:T(8,128)(2,1)S(1)} async-done(((bf16[4,128,256]{2,1,0:T(8,128)(2,1)}), bf16[4,128,256]{2,1,0:T(8,128)(2,1)S(1)}, u32[]{:S(2)}, u32[]{:S(2)}) %all-to-all-start) | async-done | bytes 262176 | tf_op jit(solution)/shard_map/all_to_all | solution.py:43
  31.9 3.0 %multiply_reduce_fusion.1 = (f32[128]{0:T(128)S(1)}, f32[128,2048]{1,0:T(8,128)S(1)}) fusion(bf16[128,1024]{0,1:T(8,128)(2,1)S(1)} %bitcast.66, bf16[1024,2048]{1,0:T(8,128)(2,1)} %param.16, bf16[128,2048]{1,0:T(8,128)(2,1)S(1)} %copy-done.1), kind=kOutput, calls=%fused_computation.32 | convolution fusion | flops 537919360 | bytes 6029824 | tf_op jit(solution)/shard_map/dot_general | solution.py:44
  35.1 5.7 %scatter_custom_fusion = bf16[256,2048]{1,0:T(8,128)(2,1)S(1)} fusion(s32[256]{0:T(256)S(1)} %bitcast.71, bf16[128,2048]{1,0:T(8,128)(2,1)S(1)} %multiply_convert_fusion, s32[1024]{0:T(1024)S(1)} %pad_clamp_fusion.1, bf16[]{:T(256)} %constant.35.clone.1), kind=kCustom, calls=%fused_computation.22 | custom fusion | bytes 1048578 | tf_op jit(solution)/shard_map/scatter | solution.py:60
  40.8 28.1 %all_to_all.34 = bf16[4,2,32,2048]{3,2,1,0:T(8,128)(2,1)S(1)} all-to-all(bf16[4,2,32,2048]{3,2,1,0:T(8,128)(2,1)S(1)} %bitcast.59), channel_id=1, replica_groups=mesh['grp'=2,'sp'=4,'tp'=4] {'sp'}, dimensions={0} | all-to-all | bytes 2097152 | tf_op jit(solution)/shard_map/all_to_all | solution.py:66
  69.6 50.7 %all_to_all.35 = bf16[4,4,1,2,32,2048]{5,4,1,3,2,0:T(8,128)(2,1)S(1)} all-to-all(bf16[4,4,1,2,32,2048]{5,4,1,3,2,0:T(8,128)(2,1)S(1)} %stack.6), channel_id=1, replica_groups=mesh['grp'=2,'sp'=4,'tp'=4] {'tp'}, dimensions={0} | all-to-all | bytes 8388608 | tf_op jit(solution)/shard_map/all_to_all | solution.py:64
  121.3 1.7 copy-done.4
  123.0 1.5 fusion.10
  124.5 1.5 fusion.5
  126.0 6.0 %convolution_convert_fusion.1 = bf16[512,2048]{1,0:T(8,128)(2,1)} fusion(bf16[512,2048]{1,0:T(8,128)(2,1)} %bitcast.63, bf16[2,256,2048]{2,1,0:T(8,128)(2,1)} %param.23, bf16[2,2048,256]{2,1,0:T(8,128)(2,1)} %param.22, f32[512,256]{1,0:T(8,128)} %fusion.10), kind=kOutput, calls=%fused_computation.6 | convolution fusion | flops 1075576832 | bytes 6815744 | tf_op jit(solution)/shard_map/dot_general | solution.py:82
  132.0 5.3 %convolution_convert_fusion = bf16[512,2048]{1,0:T(8,128)(2,1)} fusion(bf16[512,2048]{1,0:T(8,128)(2,1)S(1)} %bitcast.61, bf16[2,256,2048]{2,1,0:T(8,128)(2,1)} %param.23, bf16[2,2048,256]{2,1,0:T(8,128)(2,1)} %param.22, f32[512,256]{1,0:T(8,128)} %fusion.5), kind=kOutput, calls=%fused_computation.5 | convolution fusion | flops 1075576832 | bytes 6815744 | tf_op jit(solution)/shard_map/dot_general | solution.py:82
  137.3 4.5 %pad_maximum_fusion = bf16[4,4,2,32,2048]{4,3,1,0,2:T(8,128)(2,1)} fusion(bf16[4,4,1,32,2048]{4,3,1,0,2:T(8,128)(2,1)} %bitcast.65, bf16[4,4,1,32,2048]{4,3,1,0,2:T(8,128)(2,1)} %bitcast.64), kind=kLoop, calls=%fused_computation.3 | loop fusion | flops 2097152 | bytes 8388608 | tf_op jit(solution)/shard_map/stack | solution.py:86
  141.9 0.6 copy-done.5
  142.5 0.6 dynamic-slice
  143.1 82.6 %all-reduce.3.cloned.1.call-done = bf16[4,4,2,32,2048]{4,3,1,0,2:T(8,128)(2,1)} async-done(((bf16[4,4,2,32,2048]{4,3,1,0,2:T(8,128)(2,1)}), bf16[4,4,2,32,2048]{4,3,1,0,2:T(8,128)(2,1)}) %all-reduce.3.cloned.1.call-update) | async-done | bytes 4194320
  225.7 1.9 dynamic-slice_bitcast_fusion
  227.6 1.0 copy.38
  228.7 4.6 %all-to-all-start.3 = ((bf16[4,2,32,2048]{3,2,1,0:T(8,128)(2,1)}), bf16[4,2,32,2048]{3,2,1,0:T(8,128)(2,1)S(1)}, u32[]{:S(2)}, u32[]{:S(2)}) async-start(bf16[4,2,32,2048]{3,2,1,0:T(8,128)(2,1)} %copy.38), calls=%async_computation.3 | async-start | bytes 2097152 | tf_op jit(solution)/shard_map/all_to_all | solution.py:88
  233.4 25.3 %all-to-all-done.3 = bf16[4,2,32,2048]{3,2,1,0:T(8,128)(2,1)S(1)} async-done(((bf16[4,2,32,2048]{3,2,1,0:T(8,128)(2,1)}), bf16[4,2,32,2048]{3,2,1,0:T(8,128)(2,1)S(1)}, u32[]{:S(2)}, u32[]{:S(2)}) %all-to-all-start.3) | async-done | bytes 1048608 | tf_op jit(solution)/shard_map/all_to_all | solution.py:88
  258.7 2.3 gather_fusion
  261.0 2.4 reshape.109
  263.4 3.2 %multiply_reduce_fusion = f32[128,2048]{1,0:T(8,128)S(1)} fusion(f32[128,2,2048]{2,1,0:T(2,128)S(1)} %reshape.109, f32[128,2]{1,0:T(8,128)S(1)} %copy.33), kind=kLoop, calls=%fused_computation.8 | loop fusion | flops 786432 | bytes 3146752 | tf_op jit(solution)/shard_map/reduce_sum | solution.py:93
  266.6 0.9 add_convert_fusion
  (31 shorter events, 2.7 us)
Async XLA Ops:
  6.5 25.4 %copy-start.1 = (bf16[128,2048]{1,0:T(8,128)(2,1)S(1)}, bf16[128,2048]{1,0:T(8,128)(2,1)}, u32[]{:S(2)}) copy-start(bf16[128,2048]{1,0:T(8,128)(2,1)} %param.17) | copy-start | bytes 1572868
  7.3 13.2 %collective-permute-start = (bf16[2,256]{1,0:T(2,128)(2,1)S(1)}, bf16[2,256]{1,0:T(2,128)(2,1)S(1)}, u32[]{:S(2)}, u32[]{:S(2)}) collective-permute-start(bf16[2,256]{1,0:T(2,128)(2,1)S(1)} %slice.46), channel_id=1, source_target_pairs={{0,4},{4,8},{8,12},{1,5},{5,9},{9,13},{2,6},{6,10},{10,14},{3,7},{... | collective-permute-start | bytes 3080 | tf_op jit(solution)/shard_map/ppermute | solution.py:10
  12.9 7.5 %collective-permute-start.1 = (bf16[2,256]{1,0:T(2,128)(2,1)S(1)}, bf16[2,256]{1,0:T(2,128)(2,1)S(1)}, u32[]{:S(2)}, u32[]{:S(2)}) collective-permute-start(bf16[2,256]{1,0:T(2,128)(2,1)S(1)} %slice.47), channel_id=1, source_target_pairs={{0,4},{4,8},{8,12},{1,5},{5,9},{9,13},{2,6},{6,10},{10,14},{3,7},{... | collective-permute-start | bytes 3080 | tf_op jit(solution)/shard_map/ppermute | solution.py:10
  22.4 9.4 %all-to-all-start = ((bf16[4,128,256]{2,1,0:T(8,128)(2,1)}), bf16[4,128,256]{2,1,0:T(8,128)(2,1)S(1)}, u32[]{:S(2)}, u32[]{:S(2)}) async-start(bf16[4,128,256]{2,1,0:T(8,128)(2,1)} %bitcast.3), calls=%async_computation | async-start | bytes 524288 | tf_op jit(solution)/shard_map/all_to_all | solution.py:43
  25.8 199.9 %all-reduce.3.cloned.1.call-start = ((), (), s32[]{:S(2)}) async-start(), calls=%async_computation.4 | async-start | bytes 8388608
  31.9 3.0 %copy-start.2 = (f32[2048]{0:T(1024)S(1)}, f32[2048]{0:T(1024)}, u32[]{:S(2)}) copy-start(f32[2048]{0:T(1024)} %param.18) | copy-start | bytes 24580
  120.9 2.1 copy-start.4
  121.3 3.2 %copy-start = (bf16[4,4,1,32,2048]{4,3,1,0,2:T(8,128)(2,1)}, bf16[4,4,1,32,2048]{4,3,1,0,2:T(8,128)(2,1)S(1)}, u32[]{:S(2)}) copy-start(bf16[4,4,1,32,2048]{4,3,1,0,2:T(8,128)(2,1)S(1)} %get-tuple-element.5) | copy-start | bytes 6291460
  141.9 0.7 copy-start.5
  227.6 5.6 %copy-start.3 = (f32[128,2]{0,1:T(2,128)S(1)}, f32[128,2]{0,1:T(2,128)}, u32[]{:S(2)}) copy-start(f32[128,2]{0,1:T(2,128)} %param.20) | copy-start | bytes 3076
  228.7 30.0 %all-to-all-start.3 = ((bf16[4,2,32,2048]{3,2,1,0:T(8,128)(2,1)}), bf16[4,2,32,2048]{3,2,1,0:T(8,128)(2,1)S(1)}, u32[]{:S(2)}, u32[]{:S(2)}) async-start(bf16[4,2,32,2048]{3,2,1,0:T(8,128)(2,1)} %copy.38), calls=%async_computation.3 | async-start | bytes 2097152 | tf_op jit(solution)/shard_map/all_to_all | solution.py:88
Sparse Core Ops, SparseCore 0:
  142.0 83.6 all-reduce.2
